TPU v7x, 32 devices: a whole 2x2x4 slice. The times are simulated.
32 devices in a mesh: fs: 8 (over z, y), tp: 4 (over x, core).
Axes of the slice: x: 2, y: 2, z: 4, core: 2. Of those that a mesh axis runs over, the one named last changes fastest.
Arguments:
- tokens: bfloat16 [8192, 2048], P('fs'), may hold values from -6 to 6
- norm_gain: float32 [2048], P('fs'), may hold values from 0.1 to 1.9
- gate_train: float32 [8, 2048, 768], P(None, 'fs', 'tp'), may hold values from -0.125 to 0.125
- up_train: float32 [8, 2048, 768], P(None, 'fs', 'tp'), may hold values from -0.125 to 0.125
- down_train: float32 [8, 768, 2048], P(None, 'fs', 'tp'), may hold values from -0.21875 to 0.21875
- expert_ids: int32 [8192, 2], P('fs'), may hold values from 0 to 7, all different within a row; in each aligned block of 1024 rows (0 to 1023, 1024 to 2047, ...) at most 512 rows name the same one
- route_weights: float32 [8192, 2], P('fs'), may hold values from 0.1 to 1
Outputs:
- gate_serve: bfloat16 [8, 2048, 768], P('fs', None, 'tp')
- up_serve: bfloat16 [8, 2048, 768], P('fs', None, 'tp')
- down_serve: bfloat16 [8, 768, 2048], P('fs', 'tp')
- mixed: bfloat16 [8192, 2048], P('fs', 'tp')
Inputs may be any that keep to these rules, and one draw needn't show every extreme that they name: `expert_ids`: each row names 2 different experts. Within each aligned block of 1024 rows no expert is named more than 512 times, and in every block some expert is named exactly 512 times; every expert is named somewhere.
All inputs are finite; a program needn't handle non-finite values.
Results may differ from a plain program's by a relative error of at most 0.011.
Values may be sent and summed in bfloat16 or wider, within the bound.
A program may use at most 128 MiB of HBM per device.

v0:
```python
import functools

import jax
import jax.numpy as jnp
from jax import lax
from jax.experimental import pallas as pl
from jax.experimental.pallas import tpu as pltpu
from jax.sharding import PartitionSpec as P

epsilon = 1e-06


def gathered(tokens, norm_gain, gate_train, up_train, down_train, expert_ids, route_weights):
    experts, rows, cols = gate_train.shape
    fs_at = lax.axis_index("fs")
    tok_rows, picks = expert_ids.shape
    down_rows, down_cols = down_train.shape[1:]
    fs_count = lax.axis_size("fs")

    gate_up = jnp.concatenate(
        [norm_gain[None, :, None] * gate_train, norm_gain[None, :, None] * up_train], axis=2
    ).astype(jnp.bfloat16)
    gate_up = gate_up.transpose(1, 0, 2).reshape(rows, experts * 2 * cols)
    gate_up_all = lax.all_gather(gate_up, "fs", axis=0, tiled=True)
    down_all = lax.all_gather(
        down_train.astype(jnp.bfloat16).reshape(experts * down_rows, down_cols),
        "fs", axis=0, tiled=True,
    )

    tok_float = tokens.astype(jnp.float32)
    normed = (
        tok_float * lax.rsqrt(jnp.mean(tok_float * tok_float, axis=-1, keepdims=True) + epsilon)
    ).astype(jnp.bfloat16)
    shares = route_weights / jnp.sum(route_weights, axis=-1, keepdims=True)

    group = 2 * lax.axis_size("tp")
    picked = [jnp.zeros((tok_rows, cols), jnp.float32) for _ in range(picks)]
    for first in range(0, experts, group):
        part = gate_up_all[:, first * 2 * cols : (first + group) * 2 * cols]
        if first:
            part, picked = lax.optimization_barrier((part, picked))
        acts = jnp.dot(normed, part, preferred_element_type=jnp.float32)
        for at in range(group):
            g = acts[:, at * 2 * cols : at * 2 * cols + cols]
            u = acts[:, at * 2 * cols + cols : (at + 1) * 2 * cols]
            h = jax.nn.silu(g) * u
            for k in range(picks):
                picked[k] = picked[k] + jnp.where(
                    expert_ids[:, k : k + 1] == first + at, h, 0.0
                )
    hidden = jnp.stack([picked[k] * shares[:, k : k + 1] for k in range(picks)], 0)
    hidden_all = lax.all_gather(hidden.astype(jnp.bfloat16), "tp", axis=2, tiled=True)
    hidden_all = hidden_all.reshape(picks, tok_rows, fs_count, 1, down_rows)
    ids = jnp.arange(experts, dtype=jnp.int32)[None, None, :, None]
    mixed = jnp.zeros((tok_rows, down_cols), jnp.float32)
    for first in range(0, fs_count, group):
        blocks = hidden_all[:, :, first : first + group]
        if first:
            blocks, mixed = lax.optimization_barrier((blocks, mixed))
        spread = jnp.zeros((tok_rows, group, experts, down_rows), jnp.bfloat16)
        for k in range(picks):
            spread = jnp.where(expert_ids[:, k][:, None, None, None] == ids, blocks[k], spread)
        depth = experts * down_rows
        mixed = mixed + jnp.dot(
            spread.reshape(tok_rows, group * depth),
            down_all[first * depth : (first + group) * depth],
            preferred_element_type=jnp.float32,
        )
    mixed = mixed.astype(jnp.bfloat16)

    own = lax.dynamic_slice_in_dim(gate_up_all, fs_at * 2 * cols, 2 * cols, 1)
    down_own = lax.dynamic_slice_in_dim(
        down_all.reshape(fs_count, experts, down_rows, down_cols), fs_at, 1, 1
    ).reshape(1, fs_count * down_rows, down_cols)
    down_serve = lax.all_to_all(down_own, "tp", split_axis=1, concat_axis=2, tiled=True)
    return own[None, :, :cols], own[None, :, cols:], down_serve, mixed


def ring_kernel(
    n, tp_count, blocks, gu_ref, dn_ref, tokens_ref, ids_ref, routes_ref,
    main_ref, tail_ref, serve_ref, mixed_ref,
    gu_all, dn_all, picked, picked_all, total,
    send_sem, recv_sem, pick_send, pick_recv, serve_send, serve_recv, serve_copy, own_sem,
):
    fs_at, tp_at = lax.axis_index("fs"), lax.axis_index("tp")
    experts, down_rows, down_cols = dn_ref.shape
    rows = gu_ref.shape[1]
    tok_rows = tokens_ref.shape[0]
    half = experts // 2
    last = n // 2

    place = (1 - fs_at % 2) * (fs_at // 2) + (fs_at % 2) * (n - 1 - fs_at // 2)

    def index_at(step):
        at = (place + step + n) % n
        odd = at // last
        return (1 - odd) * (2 * at) + odd * (2 * (n - 1 - at) + 1)

    right, left = index_at(1), index_at(-1)
    barrier = pltpu.get_barrier_semaphore()
    for to in (right, left):
        pl.semaphore_signal(
            barrier, inc=1, device_id={"fs": to}, device_id_type=pl.DeviceIdType.MESH
        )
    for hop in range(1, tp_count):
        pl.semaphore_signal(
            barrier, inc=1, device_id={"tp": (tp_at + hop) % tp_count},
            device_id_type=pl.DeviceIdType.MESH,
        )
    pl.semaphore_wait(barrier, 1 + tp_count)

    def landing(unit, source):
        if unit < 2:
            return gu_all.at[unit, pl.ds(pl.multiple_of(source * rows, rows), rows), :]
        return dn_all.at[
            source // 2, pl.ds((unit - 2) * half, half),
            pl.ds(pl.multiple_of((source % 2) * down_rows, down_rows), down_rows), :,
        ]

    def message(way, step, unit):
        source = index_at(1 - step if way == 0 else step - 1)
        place_of = landing(unit, source)
        if step == 1:
            src = gu_ref.at[unit] if unit < 2 else dn_ref.at[pl.ds((unit - 2) * half, half)]
        else:
            src = place_of
        return pltpu.make_async_remote_copy(
            src_ref=src, dst_ref=place_of,
            send_sem=send_sem.at[way, step - 1, unit], recv_sem=recv_sem.at[way, step - 1, unit],
            device_id={"fs": right if way == 0 else left},
            device_id_type=pl.DeviceIdType.MESH,
        )

    started = []

    def send(way, step, unit):
        if step < last or (step == last and unit % 2 == way):
            message(way, step, unit).start()
            started.append((way, step, unit))

    def receive(way, step, unit):
        if step < last or (step == last and unit % 2 == way):
            source = index_at(-step if way == 0 else step)
            place_of = landing(unit, source)
            pltpu.make_async_remote_copy(
                src_ref=place_of, dst_ref=place_of,
                send_sem=send_sem.at[way, step - 1, unit],
                recv_sem=recv_sem.at[way, step - 1, unit],
                device_id={"fs": right if way == 0 else left},
                device_id_type=pl.DeviceIdType.MESH,
            ).wait_recv()

    def relay(step, unit):
        for way in (0, 1):
            receive(way, step, unit)
            if step < last:
                send(way, step + 1, unit)

    for unit in (0, 1):
        for way in (0, 1):
            send(way, 1, unit)
    own = [
        pltpu.make_async_copy(gu_ref.at[unit], landing(unit, fs_at), own_sem.at[unit])
        for unit in (0, 1)
    ] + [
        pltpu.make_async_copy(
            dn_ref.at[pl.ds((unit - 2) * half, half)], landing(unit, fs_at), own_sem.at[unit]
        )
        for unit in (2, 3)
    ]
    for copy in own:
        copy.start()

    serves = []

    def serve(step):
        source = index_at(step)
        to = source // 2
        src = dn_all.at[
            source // 2, fs_at,
            pl.ds(pl.multiple_of((source % 2) * down_rows, down_rows), down_rows), :,
        ]
        dst = serve_ref.at[
            pl.ds(pl.multiple_of((source % 2) * down_rows, down_rows), down_rows),
            pl.ds(pl.multiple_of(tp_at * down_cols, down_cols), down_cols),
        ]
        slot = len(serves)
        remote = pltpu.make_async_remote_copy(
            src_ref=src, dst_ref=dst, send_sem=serve_send.at[slot],
            recv_sem=serve_recv.at[source % 2, tp_at],
            device_id={"tp": to}, device_id_type=pl.DeviceIdType.MESH,
        )
        local = pltpu.make_async_copy(src, dst, serve_copy.at[slot])
        pl.when(to != tp_at)(remote.start)
        pl.when(to == tp_at)(local.start)
        serves.append((to, remote, local))

    for step in range(1, last):
        for unit in (0, 1):
            relay(step, unit)
    for unit in (2, 3):
        for way in (0, 1):
            send(way, 1, unit)
    for copy in own:
        copy.wait()
    serve(0)
    for unit in (0, 1):
        relay(last, unit)

    lane = lax.broadcasted_iota(jnp.int32, (1, 384), 1)
    parity = jnp.where(lane < 256, lane // 128, (lane - 256) // 64)
    low = lax.broadcasted_iota(jnp.int32, (1, 128), 1) < 64
    height = tok_rows // blocks
    picks = []

    def evaluate(block):
        at = block * height
        tokens = tokens_ref[pl.ds(at, height), :].astype(jnp.float32)
        square = jnp.mean(tokens * tokens, axis=-1, keepdims=True)
        tokens = (tokens * lax.rsqrt(square + epsilon)).astype(jnp.bfloat16)
        ids = [ids_ref[pl.ds(at, height), pl.ds(k, 1)] for k in (0, 1)]
        folded = [jnp.zeros((height, 384), jnp.float32) for _ in (0, 1)]
        for first in range(0, half, 2):
            span = pl.ds(first * 384, 768)
            gate = jnp.dot(tokens, gu_all[0, :, span], preferred_element_type=jnp.float32)
            up = jnp.dot(tokens, gu_all[1, :, span], preferred_element_type=jnp.float32)
            hidden = gate / (1.0 + jnp.exp(-gate)) * up
            for pair in (0, 1):
                part = hidden[:, pair * 384 : (pair + 1) * 384]
                named = 2 * (first + pair) + parity
                for k in (0, 1):
                    folded[k] = folded[k] + jnp.where(ids[k] == named, part, 0.0)
        routes = [routes_ref[pl.ds(at, height), pl.ds(k, 1)] for k in (0, 1)]
        folded = [folded[k] * (routes[k] / (routes[0] + routes[1])) for k in (0, 1)]
        ends = [f[:, 256:384] + pltpu.roll(f[:, 256:384], 64, 1) for f in folded]
        for k in (0, 1):
            main = folded[k][:, :128] + folded[k][:, 128:256]
            picked[pl.ds(at, height), pl.ds(k * 128, 128)] = main.astype(jnp.bfloat16)
        picked[pl.ds(at, height), pl.ds(256, 128)] = jnp.where(low, ends[0], ends[1]).astype(
            jnp.bfloat16
        )
        for hop in range(1, tp_count):
            copy = pltpu.make_async_remote_copy(
                src_ref=picked.at[pl.ds(at, height), :],
                dst_ref=picked_all.at[tp_at, pl.ds(at, height), :],
                send_sem=pick_send.at[hop - 1, block], recv_sem=pick_recv.at[hop - 1, block],
                device_id={"tp": (tp_at + hop) % tp_count},
                device_id_type=pl.DeviceIdType.MESH,
            )
            copy.start()
            picks.append(copy)
        picked_all[tp_at, pl.ds(at, height), :] = picked[pl.ds(at, height), :]

    events = [(step, unit) for step in range(1, last) for unit in (2, 3)]

    def event():
        step, unit = events.pop(0)
        relay(step, unit)
        if unit == 3:
            serve(-step)
            serve(step)

    for block in range(blocks):
        evaluate(block)
        if block > 0:
            event()

    main_at = pl.multiple_of((fs_at // 2) * 384 + (fs_at % 2) * 128, 128)
    tail_at = pl.multiple_of((fs_at // 2) * 384 + 256, 128)
    main_ref[...] = gu_all[:, :, pl.ds(main_at, 128)]
    tail_ref[...] = gu_all[:, :, pl.ds(tail_at, 128)]

    while events:
        event()
    for hop in range(1, tp_count):
        for block in range(blocks):
            picks[block * (tp_count - 1) + hop - 1].wait()

    def project(index, first):
        for block in range(blocks):
            at = block * height
            ids = [ids_ref[pl.ds(at, height), pl.ds(k, 1)] for k in (0, 1)]
            held = picked_all[index, pl.ds(at, height), :].astype(jnp.float32)
            end = held[:, 256:384]
            turned = pltpu.roll(end, 64, 1)
            ends = [jnp.where(low, end, turned), jnp.where(low, turned, end)]
            pieces, weights = [], []
            for pair in range(half):
                for e in (2 * pair, 2 * pair + 1):
                    pieces.append(
                        jnp.where(ids[0] == e, held[:, :128],
                                  jnp.where(ids[1] == e, held[:, 128:256], 0.0))
                    )
                    weights.append(dn_all[index, e, pl.ds(0, 128), :])
                named = 2 * pair + parity[:, 256:384]
                pieces.append(
                    jnp.where(ids[0] == named, ends[0], jnp.where(ids[1] == named, ends[1], 0.0))
                )
                for e in (2 * pair, 2 * pair + 1):
                    weights.append(dn_all[index, e, pl.ds(128, 64), :])
            spread = jnp.concatenate([p.astype(jnp.bfloat16) for p in pieces], axis=1)
            product = jnp.dot(
                spread, jnp.concatenate(weights, axis=0), preferred_element_type=jnp.float32
            )
            if first:
                total[pl.ds(at, height), :] = product
            else:
                total[pl.ds(at, height), :] += product

    far = index_at(last) // 2
    project((far + 1) % last, True)

    def middle(step, carry):
        project((far + step) % last, False)
        return carry

    lax.fori_loop(2, last, middle, 0)
    for unit in (2, 3):
        relay(last, unit)
    serve(last)
    project(far, False)
    mixed_ref[...] = total[...].astype(jnp.bfloat16)

    for way, step, unit in started:
        message(way, step, unit).wait_send()
    for to, remote, local in serves:
        pl.when(to != tp_at)(remote.wait_send)
        pl.when(to == tp_at)(local.wait)
    for part in (0, 1):
        for source in range(tp_count):
            dst = serve_ref.at[
                pl.ds(part * down_rows, down_rows), pl.ds(source * down_cols, down_cols)
            ]
            arrival = pltpu.make_async_remote_copy(
                src_ref=dst, dst_ref=dst, send_sem=serve_send.at[0],
                recv_sem=serve_recv.at[part, source],
                device_id={"tp": (tp_at + 1) % tp_count}, device_id_type=pl.DeviceIdType.MESH,
            )
            pl.when(tp_at != source)(arrival.wait_recv)


def ringed(tokens, norm_gain, gate_train, up_train, down_train, expert_ids, route_weights):
    experts, rows, cols = gate_train.shape
    down_rows, down_cols = down_train.shape[1:]
    n, tp_count = lax.axis_size("fs"), lax.axis_size("tp")
    tok_rows, width = tokens.shape
    half = experts // 2
    blocks = 4

    def paired(train):
        value = (norm_gain[None, :, None] * train).astype(jnp.bfloat16)
        value = value.transpose(1, 0, 2).reshape(rows, half, 2, cols)
        return jnp.concatenate(
            [value[..., :128].reshape(rows, half, 256), value[..., 128:].reshape(rows, half, 128)],
            axis=2,
        ).reshape(rows, half * 384)

    vmem = pl.BlockSpec(memory_space=pltpu.VMEM)
    dma = pltpu.SemaphoreType.DMA
    main, tail, serve, mixed = pl.pallas_call(
        functools.partial(ring_kernel, n, tp_count, blocks),
        out_shape=(
            jax.ShapeDtypeStruct((2, width, 128), jnp.bfloat16),
            jax.ShapeDtypeStruct((2, width, 128), jnp.bfloat16),
            jax.ShapeDtypeStruct((2 * down_rows, width), jnp.bfloat16),
            jax.ShapeDtypeStruct((tok_rows, down_cols), jnp.bfloat16),
        ),
        in_specs=[vmem] * 5,
        out_specs=(vmem,) * 4,
        scratch_shapes=[
            pltpu.VMEM((2, width, half * 384), jnp.bfloat16),
            pltpu.VMEM((n // 2, experts, 2 * down_rows, down_cols), jnp.bfloat16),
            pltpu.VMEM((tok_rows, 384), jnp.bfloat16),
            pltpu.VMEM((tp_count, tok_rows, 384), jnp.bfloat16),
            pltpu.VMEM((tok_rows, down_cols), jnp.float32),
            dma((2, n // 2, 4)),
            dma((2, n // 2, 4)),
            dma((tp_count - 1, blocks)),
            dma((tp_count - 1, blocks)),
            dma((n,)),
            dma((2, tp_count)),
            dma((n,)),
            dma((4,)),
        ],
        compiler_params=pltpu.CompilerParams(
            collective_id=0, has_side_effects=True, vmem_limit_bytes=60 * 1024 * 1024
        ),
    )(
        jnp.stack([paired(gate_train), paired(up_train)]), down_train.astype(jnp.bfloat16),
        tokens, expert_ids, route_weights,
    )
    odd = lax.axis_index("fs") % 2
    whole = jnp.concatenate(
        [main, jnp.where(odd == 1, tail[..., 64:], tail[..., :64])], axis=2
    )
    return whole[0:1], whole[1:2], serve[None], mixed


def on_device(tokens, norm_gain, gate_train, up_train, down_train, expert_ids, route_weights):
    experts, rows, cols = gate_train.shape
    n, tp_count = lax.axis_size("fs"), lax.axis_size("tp")
    fits = experts == n and n == 2 * tp_count and cols == 192 and expert_ids.shape[1] == 2
    held = 3 * experts * n * rows * cols * 2
    run = ringed if fits and held < 24 * 1024 * 1024 else gathered
    return run(
        tokens, norm_gain, gate_train, up_train, down_train, expert_ids, route_weights
    )


def solution(mesh):
    return jax.shard_map(
        on_device,
        mesh=mesh,
        in_specs=(
            P("fs", None),
            P("fs"),
            P(None, "fs", "tp"),
            P(None, "fs", "tp"),
            P(None, "fs", "tp"),
            P("fs", None),
            P("fs", None),
        ),
        out_specs=(P("fs", None, "tp"), P("fs", None, "tp"), P("fs", "tp", None), P("fs", "tp")),
        check_vma=False,
    )
```

profile of v0, /device:TPU:0, one launch (start us, length us, event | category | flops | bytes accessed | tf_op | source)
XLA Modules:
  0.0 212.6 jit_solution(9932086685451836143)
XLA Ops:
  0.6 2.2 %multiply_convert_fusion.1 = (bf16[8,256,192]{1,2,0:T(8,128)(2,1)S(1)}, bf16[8,256,192]{1,2,0:T(8,128)(2,1)S(1)}) fusion(f32[8,256,192]{1,2,0:T(8,128)} %param.9, f32[256]{0:T(256)} %param.8, f32[8,256,192]{1,2,0:T(8,128)} %param.10), kind=kLoop, calls=%fused_computation.4 | loop fusion | flops 1572864 | bytes 4719616 | tf_op jit(solution)/shard_map/convert_element_type | solution.py:351
  2.9 0.2 copy.22
  3.1 0.3 copy.21
  3.4 0.4 pad_maximum_fusion.3
  3.8 0.3 stack_reshape.7
  4.1 0.2 copy.20
  4.4 0.3 copy.19
  4.7 0.4 pad_maximum_fusion.2
  5.1 0.3 stack_reshape.6
  5.4 0.0 copy-start
  5.4 1.3 pad_maximum_fusion.gu_ref
  6.7 0.7 copy-done
  7.4 0.0 copy-start.4
  7.4 0.0 copy-start.5
  7.4 1.0 convert_element_type.11.dn_ref
  8.3 0.0 copy-done.4
  8.4 1.0 copy.23.ids_ref
  9.4 0.0 copy-done.5
  9.4 1.0 copy.24.routes_ref
  10.4 195.5 %shard_map.102 = (bf16[2,2048,128]{2,1,0:T(8,128)(2,1)}, bf16[2,2048,128]{2,1,0:T(8,128)(2,1)}, bf16[192,2048]{1,0:T(8,128)(2,1)}, bf16[1024,512]{1,0:T(8,128)(2,1)}) custom-call(bf16[2,256,1536]{2,1,0:T(8,128)(2,1)} %pad_maximum_fusion.gu_ref, bf16[8,96,512]{2,1,0:T(8,128)(2,1)} %convert_element_type.11.dn_ref, bf16[1024,2048]{1,0:T(8,128)(2,1)} %tokens_ref.1, ...), custom_call_target="tpu_custom_call" | custom-call | tf_op jit(solution)/shard_map/pallas_call | solution.py:360
  205.9 0.0 copy-start.2
  205.9 2.0 slice_select_fusion
  207.9 0.0 copy-done.2
  207.9 0.4 pad_maximum_fusion.1
  208.3 0.0 copy-start.3
  208.3 1.2 copy.25
  209.5 0.0 copy-start.1
  209.6 1.2 copy.26
  210.8 0.0 copy-done.3
  210.8 0.9 copy.29
  211.7 0.0 copy-done.1
  211.7 1.0 copy.30
  (4 shorter events, 0.1 us)
Async XLA Ops:
  5.4 2.0 copy-start
  7.4 1.0 copy-start.4
  7.4 2.0 copy-start.5
  205.9 2.0 copy-start.2
  208.3 2.5 %copy-start.3 = (bf16[192,2048]{1,0:T(8,128)(2,1)S(1)}, bf16[192,2048]{1,0:T(8,128)(2,1)}, u32[]{:S(2)}) copy-start(bf16[192,2048]{1,0:T(8,128)(2,1)} %get-tuple-element.10) | copy-start | bytes 2359300
  209.5 2.1 copy-start.1
where the time goes:
time: 213 us
  Pallas kernels  195 us (92%)
  local copies, waits for them, and re-layouts  8.71 us (4%)
  other arithmetic  7.66 us (4%)
    pallas_call x1, Pallas kernels, ringed(): pl.pallas_call(functools.partial(ring_kernel, n, tp_count, blocks), out_s...  195 us
    unnamed x18, local copies, waits for them, and re-layouts  7.06 us

commit v1 on v0

v1 whole, which is shorter than its diff:
```python
import functools

import jax
import jax.numpy as jnp
from jax import lax
from jax.experimental import pallas as pl
from jax.experimental.pallas import tpu as pltpu
from jax.sharding import PartitionSpec as P

epsilon = 1e-06


def gathered(tokens, norm_gain, gate_train, up_train, down_train, expert_ids, route_weights):
    experts, rows, cols = gate_train.shape
    fs_at = lax.axis_index("fs")
    tok_rows, picks = expert_ids.shape
    down_rows, down_cols = down_train.shape[1:]
    fs_count = lax.axis_size("fs")

    gate_up = jnp.concatenate(
        [norm_gain[None, :, None] * gate_train, norm_gain[None, :, None] * up_train], axis=2
    ).astype(jnp.bfloat16)
    gate_up = gate_up.transpose(1, 0, 2).reshape(rows, experts * 2 * cols)
    gate_up_all = lax.all_gather(gate_up, "fs", axis=0, tiled=True)
    down_all = lax.all_gather(
        down_train.astype(jnp.bfloat16).reshape(experts * down_rows, down_cols),
        "fs", axis=0, tiled=True,
    )

    tok_float = tokens.astype(jnp.float32)
    normed = (
        tok_float * lax.rsqrt(jnp.mean(tok_float * tok_float, axis=-1, keepdims=True) + epsilon)
    ).astype(jnp.bfloat16)
    shares = route_weights / jnp.sum(route_weights, axis=-1, keepdims=True)

    group = 2 * lax.axis_size("tp")
    picked = [jnp.zeros((tok_rows, cols), jnp.float32) for _ in range(picks)]
    for first in range(0, experts, group):
        part = gate_up_all[:, first * 2 * cols : (first + group) * 2 * cols]
        if first:
            part, picked = lax.optimization_barrier((part, picked))
        acts = jnp.dot(normed, part, preferred_element_type=jnp.float32)
        for at in range(group):
            g = acts[:, at * 2 * cols : at * 2 * cols + cols]
            u = acts[:, at * 2 * cols + cols : (at + 1) * 2 * cols]
            h = jax.nn.silu(g) * u
            for k in range(picks):
                picked[k] = picked[k] + jnp.where(
                    expert_ids[:, k : k + 1] == first + at, h, 0.0
                )
    hidden = jnp.stack([picked[k] * shares[:, k : k + 1] for k in range(picks)], 0)
    hidden_all = lax.all_gather(hidden.astype(jnp.bfloat16), "tp", axis=2, tiled=True)
    hidden_all = hidden_all.reshape(picks, tok_rows, fs_count, 1, down_rows)
    ids = jnp.arange(experts, dtype=jnp.int32)[None, None, :, None]
    mixed = jnp.zeros((tok_rows, down_cols), jnp.float32)
    for first in range(0, fs_count, group):
        blocks = hidden_all[:, :, first : first + group]
        if first:
            blocks, mixed = lax.optimization_barrier((blocks, mixed))
        spread = jnp.zeros((tok_rows, group, experts, down_rows), jnp.bfloat16)
        for k in range(picks):
            spread = jnp.where(expert_ids[:, k][:, None, None, None] == ids, blocks[k], spread)
        depth = experts * down_rows
        mixed = mixed + jnp.dot(
            spread.reshape(tok_rows, group * depth),
            down_all[first * depth : (first + group) * depth],
            preferred_element_type=jnp.float32,
        )
    mixed = mixed.astype(jnp.bfloat16)

    own = lax.dynamic_slice_in_dim(gate_up_all, fs_at * 2 * cols, 2 * cols, 1)
    down_own = lax.dynamic_slice_in_dim(
        down_all.reshape(fs_count, experts, down_rows, down_cols), fs_at, 1, 1
    ).reshape(1, fs_count * down_rows, down_cols)
    down_serve = lax.all_to_all(down_own, "tp", split_axis=1, concat_axis=2, tiled=True)
    return own[None, :, :cols], own[None, :, cols:], down_serve, mixed


def ladder_kernel(
    n, tp_count, parts, ahead, blocks, gu_ref, dn_ref, tokens_ref, meta_ref,
    serve_g, serve_u, serve_d, mixed_ref,
    gu_all, dn_all, far_tokens, far_meta, cols, fold, picks, total, reply, answer,
    send_sem, recv_sem, tok_send, tok_recv, meta_send, meta_recv,
    pick_send, pick_recv, reply_send, reply_recv, serve_send, serve_recv,
):
    fs_at, tp_at = lax.axis_index("fs"), lax.axis_index("tp")
    rows = gu_ref.shape[1]
    width = gu_ref.shape[2]
    down_rows, down_cols = dn_ref.shape[2:]
    tok_rows = tokens_ref.shape[0]
    height = tok_rows // blocks
    quarter = n // 4
    base = (quarter, 2 * quarter, 0, 3 * quarter)
    gates = 4 * parts
    units = 6 * parts
    chunk = rows // parts

    z, y = fs_at // 2, fs_at % 2
    side = z // 2
    mid = jnp.logical_or(z == 1, z == 2)
    end = jnp.logical_not(mid)
    near_mid, far_mid = 1 + side, 2 - side
    near_end, far_end = 3 * side, 3 - 3 * side

    def at(zz, yy):
        return zz * 2 + yy

    E, Eo = at(near_end, y), at(near_end, 1 - y)
    M, R = at(near_mid, y), at(near_mid, 1 - y)
    X, Xo = at(far_mid, y), at(far_mid, 1 - y)
    F, Fo = at(far_end, y), at(far_end, 1 - y)
    across = tp_at + 2 - 4 * (tp_at // 2)
    mate = tp_at + 1 - 2 * (tp_at % 2)
    diagonal = across + 1 - 2 * (tp_at % 2)

    MESH = pl.DeviceIdType.MESH
    barrier = pltpu.get_barrier_semaphore()

    def greet(to):
        pl.semaphore_signal(barrier, inc=1, device_id=to, device_id_type=MESH)

    for hop in range(1, tp_count):
        greet({"tp": (tp_at + hop) % tp_count})

    @pl.when(mid)
    def _():
        greet({"fs": E})
        greet({"fs": R})
        greet({"fs": X})
        pl.semaphore_wait(barrier, tp_count + 2)

    @pl.when(end)
    def _():
        greet({"fs": M})
        greet({"fs": Eo})
        pl.semaphore_wait(barrier, tp_count + 1)

    def gu_view(u, s):
        return gu_all.at[u // parts, pl.ds(pl.multiple_of(s * rows + (u % parts) * chunk, chunk), chunk), :]

    def gu_own(u):
        return gu_ref.at[u // parts, pl.ds(pl.multiple_of((u % parts) * chunk, chunk), chunk), :]

    def dn_view(u, s):
        v = u - gates
        span = pl.ds(pl.multiple_of((s % 2) * down_rows, down_rows), down_rows)
        if parts == 4:
            return dn_all.at[v // 2, s // 2, v % 2, span, :]
        return dn_all.at[v, s // 2, :, span, :]

    def dn_own(u):
        v = u - gates
        return dn_ref.at[v // 2, v % 2] if parts == 4 else dn_ref.at[v]

    def copy(view, u, s, to, slot, src=None):
        place = view(u, s)
        return pltpu.make_async_remote_copy(
            src_ref=place if src is None else src, dst_ref=place,
            send_sem=send_sem.at[slot, u], recv_sem=recv_sem.at[s, u],
            device_id={"fs": to}, device_id_type=MESH,
        )

    def group(u, body):
        @pl.when(jnp.logical_and(u >= 0, u < gates))
        def _():
            body(u, gu_view, gu_own, u >= 2 * parts)

        @pl.when(jnp.logical_and(u >= gates, u < units))
        def _():
            body(u, dn_view, dn_own, u >= 5 * parts)

    def sends(u):
        def from_mid(u, view, own, wide):
            copy(view, u, fs_at, R, 0, own(u)).start()
            copy(view, u, fs_at, X, 3, own(u)).start()
            pl.when(wide)(lambda: copy(view, u, fs_at, E, 6, own(u)).start())

        def from_end(u, view, own, wide):
            copy(view, u, fs_at, M, 0, own(u)).start()
            copy(view, u, fs_at, Eo, 2, own(u)).start()

        pl.when(mid)(lambda: group(u, from_mid))
        pl.when(end)(lambda: group(u, from_end))

    def got(view, u, s):
        copy(view, u, s, s, 0).wait_recv()

    token_parts = 2 * parts
    token_rows = tok_rows // tp_count // token_parts
    token_from = 1

    def token_copy(j, owner, kind, to):
        span = pl.ds(pl.multiple_of((owner * token_parts + j) * token_rows, token_rows), token_rows)
        return pltpu.make_async_remote_copy(
            src_ref=tokens_ref.at[span] if kind == 0 else far_tokens.at[span],
            dst_ref=far_tokens.at[span],
            send_sem=tok_send.at[max(kind - 1, 0), j], recv_sem=tok_recv.at[owner, j],
            device_id=to, device_id_type=MESH,
        )

    def tick(t):
        sends(t + ahead)

        @pl.when(mid)
        def _():
            def first(u, view, own, wide):
                got(view, u, E)
                copy(view, u, E, X, 4).start()
                got(view, u, X)
                copy(view, u, X, R, 1).start()
                pl.when(wide)(lambda: copy(view, u, X, E, 7).start())
                got(view, u, R)

            def second(u, view, own, wide):
                got(view, u, Eo)
                pl.when(u % 2 == 1)(lambda: copy(view, u, Eo, X, 5).start())
                got(view, u, F)
                pl.when(u % 2 == 0)(lambda: copy(view, u, F, R, 2).start())
                pl.when(wide)(lambda: copy(view, u, F, E, 8).start())
                got(view, u, Xo)

            group(t, first)
            group(t - 1, second)
            group(t - 2, lambda u, view, own, wide: got(view, u, Fo))
            j = t - token_from - 1

            @pl.when(jnp.logical_and(j >= 0, j < token_parts))
            def _():
                token_copy(j, tp_at, 1, {"tp": across}).wait_recv()
                token_copy(j, tp_at, 1, {"tp": across}).start()
                token_copy(j, tp_at, 2, {"tp": mate}).start()

            i = j - 1

            @pl.when(jnp.logical_and(i >= 0, i < token_parts))
            def _():
                token_copy(i, across, 3, {"tp": mate}).wait_recv()
                token_copy(i, across, 3, {"tp": mate}).start()

        @pl.when(end)
        def _():
            def first(u, view, own, wide):
                got(view, u, Eo)
                copy(view, u, Eo, M, 1).start()

                @pl.when(wide)
                def _():
                    got(view, u, M)
                    copy(view, u, M, Eo, 3).start()

            def second(u, view, own, wide):
                @pl.when(wide)
                def _():
                    got(view, u, X)
                    copy(view, u, X, Eo, 4).start()
                    got(view, u, R)

            def third(u, view, own, wide):
                @pl.when(wide)
                def _():
                    got(view, u, F)
                    copy(view, u, F, Eo, 5).start()
                    got(view, u, Xo)

            def fourth(u, view, own, wide):
                pl.when(wide)(lambda: got(view, u, Fo))

            group(t, first)
            group(t - 1, second)
            group(t - 2, third)
            group(t - 3, fourth)
            j = t - token_from

            @pl.when(jnp.logical_and(j >= 0, j < token_parts))
            def _():
                token_copy(j, tp_at, 0, {"fs": M}).start()

    meta_copy = pltpu.make_async_remote_copy(
        src_ref=meta_ref, dst_ref=far_meta, send_sem=meta_send, recv_sem=meta_recv,
        device_id={"fs": M}, device_id_type=MESH,
    )

    def loop(first, last, body):
        def step(t, carry):
            body(t)
            return carry

        lax.fori_loop(first, last, step, 0)

    loop(0, ahead, sends)
    pl.when(end)(meta_copy.start)
    gu_all[:, pl.ds(pl.multiple_of(fs_at * rows, rows), rows), :] = gu_ref[...]
    dn_all[:, fs_at // 2, :, pl.ds(pl.multiple_of((fs_at % 2) * down_rows, down_rows), down_rows), :] = dn_ref[...]

    def columns(which, ref):
        for b in range(tok_rows // 128):
            cols[which, pl.ds(b * 128, 128), :] = jnp.transpose(ref[:, pl.ds(b * 128, 128)])

    columns(0, meta_ref)

    lane = lax.broadcasted_iota(jnp.int32, (1, 384), 1)
    parity = jnp.where(lane < 256, lane // 128, (lane - 256) // 64).astype(jnp.float32)
    low = lax.broadcasted_iota(jnp.int32, (1, 128), 1) < 64

    def span_of(block):
        return pl.ds(pl.multiple_of(block * height, height), height)

    def evaluate(block, ref, which, phase):
        span = span_of(block)
        tokens = ref[span, :].astype(jnp.float32)
        square = jnp.mean(tokens * tokens, axis=-1, keepdims=True)
        tokens = (tokens * lax.rsqrt(square + epsilon)).astype(jnp.bfloat16)
        ids = [cols[which, span, pl.ds(k, 1)] for k in (0, 1)]
        gate = jnp.dot(tokens, gu_all[2 * phase], preferred_element_type=jnp.float32)
        up = jnp.dot(tokens, gu_all[2 * phase + 1], preferred_element_type=jnp.float32)
        hidden = gate / (1.0 + jnp.exp(-gate)) * up
        folded = []
        for k in (0, 1):
            value = jnp.zeros((height, 384), jnp.float32)
            for pair in (0, 1):
                named = base[2 * phase + pair] + parity
                part = hidden[:, pair * 384 : (pair + 1) * 384]
                value = value + jnp.where(ids[k] == named, part, 0.0)
            folded.append(value)
        return folded

    def pick_copy(block, which, owner, kind, to):
        place = picks.at[which, owner, span_of(block), :]
        return pltpu.make_async_remote_copy(
            src_ref=place, dst_ref=place,
            send_sem=pick_send.at[which, kind, block], recv_sem=pick_recv.at[which, owner, block],
            device_id={"tp": to}, device_id_type=MESH,
        )

    def share(block, which, folded):
        span = span_of(block)
        routes = [cols[which, span, pl.ds(2 + k, 1)] for k in (0, 1)]
        folded = [folded[k] * (routes[k] / (routes[0] + routes[1])) for k in (0, 1)]
        ends = [f[:, 256:384] + pltpu.roll(f[:, 256:384], 64, 1) for f in folded]
        for k in (0, 1):
            whole = folded[k][:, :128] + folded[k][:, 128:256]
            picks[which, tp_at, span, pl.ds(k * 128, 128)] = whole.astype(jnp.bfloat16)
        picks[which, tp_at, span, pl.ds(256, 128)] = jnp.where(low, ends[0], ends[1]).astype(
            jnp.bfloat16
        )
        pick_copy(block, which, tp_at, 0, across).start()
        pick_copy(block, which, tp_at, 1, mate).start()

    def pass_on(block, which):
        pick_copy(block, which, across, 2, mate).wait_recv()
        pick_copy(block, which, across, 2, mate).start()

    def picked_up(block, which):
        pick_copy(block, which, mate, 0, mate).wait_recv()
        pick_copy(block, which, diagonal, 0, mate).wait_recv()

    def project(block, which, phase):
        span = span_of(block)
        ids = [cols[which, span, pl.ds(k, 1)] for k in (0, 1)]
        product = None
        for index in range(tp_count):
            held = picks[which, index, span, :].astype(jnp.float32)
            tail = held[:, 256:384]
            turned = pltpu.roll(tail, 64, 1)
            ends = [jnp.where(low, tail, turned), jnp.where(low, turned, tail)]
            pieces, weights = [], []
            for pair in (2 * phase, 2 * phase + 1):
                for e in (0, 1):
                    named = float(base[pair] + e)
                    pieces.append(
                        jnp.where(ids[0] == named, held[:, :128],
                                  jnp.where(ids[1] == named, held[:, 128:256], 0.0))
                    )
                    weights.append(dn_all[pair, index, e, pl.ds(0, 128), :])
                named = base[pair] + parity[:, 256:384]
                pieces.append(
                    jnp.where(ids[0] == named, ends[0], jnp.where(ids[1] == named, ends[1], 0.0))
                )
                for e in (0, 1):
                    weights.append(dn_all[pair, index, e, pl.ds(128, 64), :])
            spread = jnp.concatenate([p.astype(jnp.bfloat16) for p in pieces], axis=1)
            part = jnp.dot(
                spread, jnp.concatenate(weights, axis=0), preferred_element_type=jnp.float32
            )
            product = part if product is None else product + part
        return product

    def reply_copy(block):
        return pltpu.make_async_remote_copy(
            src_ref=reply.at[span_of(block)], dst_ref=answer.at[span_of(block)],
            send_sem=reply_send.at[block], recv_sem=reply_recv.at[block],
            device_id={"fs": E}, device_id_type=MESH,
        )

    start = 2 * parts + 2
    loop(0, start, tick)

    @pl.when(end)
    def _():
        fold[...] = jnp.zeros_like(fold)

    @pl.when(mid)
    def _():
        meta_copy.wait_recv()
        columns(1, far_meta)

    def own_first(t):
        tick(t)

        @pl.when(mid)
        def _():
            folded = evaluate(t - start, tokens_ref, 0, 0)
            span = span_of(t - start)
            for k in (0, 1):
                fold[k, span, :] = folded[k]

    loop(start, start + blocks, own_first)
    start = start + blocks

    @pl.when(mid)
    def _():
        def landed(j):
            token_copy(j, mate, 1, {"tp": mate}).wait_recv()
            token_copy(j, diagonal, 1, {"tp": mate}).wait_recv()

        loop(0, token_parts, landed)

    def far_first(t):
        tick(t)

        @pl.when(mid)
        def _():
            share(t - start, 1, evaluate(t - start, far_tokens, 1, 0))

    loop(start, start + blocks, far_first)
    start = start + blocks
    ready = max(start, gates + 3)
    loop(start, ready, tick)
    start = ready

    def served(part):
        span = pl.ds(pl.multiple_of(part * rows, rows), rows)
        phase = jnp.where(mid, 0, 1)
        for kind, out in ((0, serve_g), (1, serve_u)):
            out[span, pl.ds(0, 128)] = gu_all[
                2 * phase + kind, span, pl.ds(pl.multiple_of(side * 384 + y * 128, 128), 128)
            ]
            tail = gu_all[
                2 * phase + kind, span, pl.ds(pl.multiple_of(side * 384 + 256, 128), 128)
            ].astype(jnp.float32)
            tail = jnp.where(y == 1, pltpu.roll(tail, 64, 1), tail)
            out[span, pl.ds(128, 64)] = tail[:, :64].astype(jnp.bfloat16)

    def own_second(t):
        tick(t)
        block = t - start
        folded = evaluate(block, tokens_ref, 0, 1)
        span = span_of(block)
        share(block, 0, [folded[k] + fold[k, span, :] for k in (0, 1)])
        pl.when(mid)(lambda: pass_on(block, 1))

    loop(start, start + blocks, own_second)
    start = start + blocks

    def far_second(t):
        tick(t)
        block = t - start
        pass_on(block, 0)

        @pl.when(mid)
        def _():
            picked_up(block, 1)
            reply[span_of(block)] = project(block, 1, 0).astype(jnp.bfloat16)
            reply_copy(block).start()

    loop(start, start + blocks, far_second)
    start = start + blocks
    loop(start, max(start, units + 3), tick)

    pair = jnp.where(mid, side, 2 + side)

    def serve_copy(to, owner):
        return pltpu.make_async_remote_copy(
            src_ref=dn_all.at[pair, to, y],
            dst_ref=serve_d.at[:, pl.ds(pl.multiple_of(owner * down_cols, down_cols), down_cols)],
            send_sem=serve_send.at[to], recv_sem=serve_recv.at[owner],
            device_id={"tp": to}, device_id_type=MESH,
        )

    for hop in range(1, tp_count):
        serve_copy((tp_at + hop) % tp_count, tp_at).start()
    serve_d[:, pl.ds(pl.multiple_of(tp_at * down_cols, down_cols), down_cols)] = dn_all[pair, tp_at, y]
    loop(0, n, served)

    def finish(block):
        span = span_of(block)
        picked_up(block, 0)

        @pl.when(mid)
        def _():
            total[span, :] = project(block, 0, 0)

        @pl.when(end)
        def _():
            reply_copy(block).wait_recv()
            total[span, :] = answer[span, :].astype(jnp.float32)

        mixed_ref[span, :] = (total[span, :] + project(block, 0, 1)).astype(jnp.bfloat16)

    loop(0, blocks, finish)

    def drained(u):
        def from_mid(u, view, own, wide):
            for slot in (0, 1, 3, 4):
                copy(view, u, fs_at, X, slot).wait_send()
            pl.when(u % 2 == 0)(lambda: copy(view, u, fs_at, X, 2).wait_send())
            pl.when(u % 2 == 1)(lambda: copy(view, u, fs_at, X, 5).wait_send())

            @pl.when(wide)
            def _():
                for slot in (6, 7, 8):
                    copy(view, u, fs_at, X, slot).wait_send()

        def from_end(u, view, own, wide):
            for slot in (0, 1, 2):
                copy(view, u, fs_at, M, slot).wait_send()

            @pl.when(wide)
            def _():
                for slot in (3, 4, 5):
                    copy(view, u, fs_at, M, slot).wait_send()

        pl.when(mid)(lambda: group(u, from_mid))
        pl.when(end)(lambda: group(u, from_end))

    loop(0, units, drained)

    @pl.when(mid)
    def _():
        def token_drain(j):
            for kind in (1, 2, 3):
                token_copy(j, tp_at, kind, {"tp": mate}).wait_send()

        loop(0, token_parts, token_drain)

        def block_drain(b):
            reply_copy(b).wait_send()
            for kind in (0, 1, 2):
                pick_copy(b, 1, tp_at, kind, mate).wait_send()

        loop(0, blocks, block_drain)

    @pl.when(end)
    def _():
        meta_copy.wait_send()
        loop(0, token_parts, lambda j: token_copy(j, tp_at, 0, {"fs": M}).wait_send())

    def own_drain(b):
        for kind in (0, 1, 2):
            pick_copy(b, 0, tp_at, kind, mate).wait_send()

    loop(0, blocks, own_drain)
    for hop in range(1, tp_count):
        to = (tp_at + hop) % tp_count
        serve_copy(to, tp_at).wait_send()
        serve_copy(tp_at, to).wait_recv()


def laddered(tokens, norm_gain, gate_train, up_train, down_train, expert_ids, route_weights):
    experts, rows, cols = gate_train.shape
    down_rows, down_cols = down_train.shape[1:]
    n, tp_count = lax.axis_size("fs"), lax.axis_size("tp")
    tok_rows, width = tokens.shape
    half, quarter = experts // 2, experts // 4
    blocks, parts, ahead = 4, 4, 3

    def paired(train):
        value = (norm_gain[None, :, None] * train).astype(jnp.bfloat16)
        value = jnp.concatenate([value[quarter:-quarter], value[:quarter], value[-quarter:]], axis=0)
        value = value.transpose(1, 0, 2).reshape(rows, 2, 2, 2, cols)
        value = jnp.concatenate(
            [value[..., :128].reshape(rows, 2, 2, 256), value[..., 128:].reshape(rows, 2, 2, 128)],
            axis=3,
        )
        return value.transpose(1, 0, 2, 3).reshape(2, rows, 768)

    gate, up = paired(gate_train), paired(up_train)
    gu = jnp.stack([gate, up], axis=1).reshape(4, rows, 768)
    down = down_train.astype(jnp.bfloat16)
    down = jnp.concatenate([down[quarter:-quarter], down[:quarter], down[-quarter:]], axis=0)
    down = down.reshape(4, 2, down_rows, down_cols)
    meta = jnp.concatenate(
        [expert_ids.T.astype(jnp.float32), route_weights.T, jnp.zeros((4, tok_rows), jnp.float32)],
        axis=0,
    )
    vmem = pl.BlockSpec(memory_space=pltpu.VMEM)
    dma = pltpu.SemaphoreType.DMA
    bf16, f32 = jnp.bfloat16, jnp.float32
    units = 6 * parts
    gate_serve, up_serve, down_serve, mixed = pl.pallas_call(
        functools.partial(ladder_kernel, n, tp_count, parts, ahead, blocks),
        out_shape=(
            jax.ShapeDtypeStruct((width, cols), bf16),
            jax.ShapeDtypeStruct((width, cols), bf16),
            jax.ShapeDtypeStruct((2 * down_rows, width), bf16),
            jax.ShapeDtypeStruct((tok_rows, down_cols), bf16),
        ),
        in_specs=[vmem] * 4,
        out_specs=(vmem,) * 4,
        scratch_shapes=[
            pltpu.VMEM((4, width, 768), bf16),
            pltpu.VMEM((4, tp_count, 2, 2 * down_rows, down_cols), bf16),
            pltpu.VMEM((tok_rows, width), bf16),
            pltpu.VMEM((8, tok_rows), f32),
            pltpu.VMEM((2, tok_rows, 8), f32),
            pltpu.VMEM((2, tok_rows, 384), f32),
            pltpu.VMEM((2, tp_count, tok_rows, 384), bf16),
            pltpu.VMEM((tok_rows, down_cols), f32),
            pltpu.VMEM((tok_rows, down_cols), bf16),
            pltpu.VMEM((tok_rows, down_cols), bf16),
            dma((9, units)),
            dma((n, units)),
            dma((3, 2 * parts)),
            dma((tp_count, 2 * parts)),
            dma,
            dma,
            dma((2, 3, blocks)),
            dma((2, tp_count, blocks)),
            dma((blocks,)),
            dma((blocks,)),
            dma((tp_count,)),
            dma((tp_count,)),
        ],
        compiler_params=pltpu.CompilerParams(
            collective_id=0, has_side_effects=True, vmem_limit_bytes=63 * 1024 * 1024
        ),
    )(gu, down, tokens, meta)
    return gate_serve[None], up_serve[None], down_serve[None], mixed


def on_device(tokens, norm_gain, gate_train, up_train, down_train, expert_ids, route_weights):
    experts, rows, cols = gate_train.shape
    n, tp_count = lax.axis_size("fs"), lax.axis_size("tp")
    fits = experts == n and n == 2 * tp_count and cols == 192 and expert_ids.shape[1] == 2
    held = 3 * experts * n * rows * cols * 2
    run = laddered if fits and held < 24 * 1024 * 1024 else gathered
    return run(
        tokens, norm_gain, gate_train, up_train, down_train, expert_ids, route_weights
    )


def solution(mesh):
    return jax.shard_map(
        on_device,
        mesh=mesh,
        in_specs=(
            P("fs", None),
            P("fs"),
            P(None, "fs", "tp"),
            P(None, "fs", "tp"),
            P(None, "fs", "tp"),
            P("fs", None),
            P("fs", None),
        ),
        out_specs=(P("fs", None, "tp"), P("fs", None, "tp"), P("fs", "tp", None), P("fs", "tp")),
        check_vma=False,
    )
```

time: 213 us -> 209 us (0.981)
  Pallas kernels: 195 us -> 191 us
    pallas_call x1, Pallas kernels: 195 us -> 191 us  [laddered(): pl.pallas_call(functools.partial(ladder_kernel, n, tp_count, parts, ahead...]
    unnamed x18 -> x16, local copies, waits for them, and re-layouts: 7.06 us -> 6.51 us
where the time goes in v1:
time: 209 us
  Pallas kernels  191 us (91%)
  local copies, waits for them, and re-layouts  9.09 us (4%)
  other arithmetic  7.95 us (4%)
    pallas_call x1, Pallas kernels, laddered(): pl.pallas_call(functools.partial(ladder_kernel, n, tp_count, parts, ahead...  191 us
    unnamed x16, local copies, waits for them, and re-layouts  6.51 us

profile of v1, /device:TPU:0, one launch (start us, length us, event | category | flops | bytes accessed | tf_op | source)
XLA Modules:
  0.0 208.6 jit_solution(8810889723024152193)
XLA Ops:
  0.6 0.1 pad.2.clone
  0.7 0.7 convert_bitcast_fusion
  1.4 1.4 maximum_maximum_fusion.meta_ref
  2.8 1.5 convert_element_type.17
  4.3 0.0 copy-start
  4.3 0.0 copy-start.1
  4.3 0.0 copy-start.5
  4.4 1.0 pad_maximum_fusion.3
  5.4 0.6 copy-done
  6.0 0.5 copy-done.1
  6.5 0.0 copy-done.5
  6.5 0.3 multiply_convert_fusion.1
  6.9 0.1 fusion.1
  7.0 0.1 pad_maximum_fusion.1
  7.1 0.5 copy.11
  7.6 0.2 copy.12
  7.8 0.8 maximum_bitcast_fusion
  8.6 0.5 stack_reshape.6
  9.1 0.1 pad_maximum_fusion.2
  9.2 0.5 copy.13
  9.7 0.2 copy.14
  9.9 0.8 maximum_bitcast_fusion.1
  10.7 0.5 stack_reshape.7
  11.2 1.3 pad_maximum_fusion
  12.5 190.7 %shard_map.102 = (bf16[2048,192]{1,0:T(8,128)(2,1)}, bf16[2048,192]{1,0:T(8,128)(2,1)}, bf16[192,2048]{1,0:T(8,128)(2,1)}, bf16[1024,512]{1,0:T(8,128)(2,1)}) custom-call(bf16[4,256,768]{2,1,0:T(8,128)(2,1)} %bitcast.22, bf16[4,2,96,512]{3,2,1,0:T(8,128)(2,1)} %bitcast.23, bf16[1024,2048]{1,0:T(8,128)(2,1)} %tokens_ref.1, f32[8,1024]{1,0:T(8,128)} %maximum_maximum_fusion.meta_ref), custom_call_target="tpu_custom_call" | custom-call | tf_op jit(solution)/shard_map/pallas_call | solution.py:600
  203.1 0.0 copy-start.2
  203.2 2.3 %copy.15 = bf16[1,2048,192]{1,2,0:T(8,128)(2,1)} copy(bf16[1,2048,192]{2,1,0:T(8,128)(2,1)} %bitcast.31) | data formatting | bytes 1572864
  205.5 0.0 copy-done.2
  205.5 1.2 copy.16
  206.7 0.0 copy-done.4
  206.7 0.9 copy.19
  207.6 1.0 copy.20
  (12 shorter events, 0.2 us)
Async XLA Ops:
  4.3 1.7 copy-start
  4.3 2.2 %copy-start.1 = (f32[8,256,192]{1,2,0:T(8,128)S(1)}, f32[8,256,192]{1,2,0:T(8,128)}, u32[]{:S(2)}) copy-start(f32[8,256,192]{1,2,0:T(8,128)} %param.10) | copy-start | bytes 4718596
  4.3 2.1 %copy-start.5 = (f32[256]{0:T(256)S(1)}, f32[256]{0:T(256)}, u32[]{:S(2)}) copy-start(f32[256]{0:T(256)} %param.8) | copy-start | bytes 3076
  203.1 2.3 %copy-start.2 = (bf16[2048,192]{1,0:T(8,128)(2,1)S(1)}, bf16[2048,192]{1,0:T(8,128)(2,1)}, u32[]{:S(2)}) copy-start(bf16[2048,192]{1,0:T(8,128)(2,1)} %get-tuple-element.9) | copy-start | bytes 2359300
  203.2 3.6 %copy-start.4 = (bf16[192,2048]{1,0:T(8,128)(2,1)S(1)}, bf16[192,2048]{1,0:T(8,128)(2,1)}, u32[]{:S(2)}) copy-start(bf16[192,2048]{1,0:T(8,128)(2,1)} %get-tuple-element.10) | copy-start | bytes 2359300
  205.5 2.1 %copy-start.3 = (bf16[1024,512]{1,0:T(8,128)(2,1)S(1)}, bf16[1024,512]{1,0:T(8,128)(2,1)}, u32[]{:S(2)}) copy-start(bf16[1024,512]{1,0:T(8,128)(2,1)} %get-tuple-element.33) | copy-start | bytes 3145732

commit v2 on v1

--- a/solution.py
+++ b/solution.py
@@ -77,23 +77,22 @@
 
 
 def ladder_kernel(
-    n, tp_count, parts, ahead, blocks, gu_ref, dn_ref, tokens_ref, meta_ref,
-    serve_g, serve_u, serve_d, mixed_ref,
-    gu_all, dn_all, far_tokens, far_meta, cols, fold, picks, total, reply, answer,
+    n, tp_count, parts, ahead, lag, blocks, gate_in, up_in, down_in, gain_ref, tokens_in, ids_ref,
+    routes_ref, serve_g, serve_u, serve_d, mixed_ref,
+    gate_stage, up_stage, down_stage, tokens_ref, meta_ref, stage_sem, gu_all, dn_all, far_tokens, far_meta, cols, fold, picks, total, reply, answer,
     send_sem, recv_sem, tok_send, tok_recv, meta_send, meta_recv,
     pick_send, pick_recv, reply_send, reply_recv, serve_send, serve_recv,
 ):
     fs_at, tp_at = lax.axis_index("fs"), lax.axis_index("tp")
-    rows = gu_ref.shape[1]
-    width = gu_ref.shape[2]
-    down_rows, down_cols = dn_ref.shape[2:]
-    tok_rows = tokens_ref.shape[0]
+    rows = gate_in.shape[2]
+    down_rows, down_cols = down_in.shape[1:]
+    tok_rows = tokens_in.shape[0]
     height = tok_rows // blocks
     quarter = n // 4
     base = (quarter, 2 * quarter, 0, 3 * quarter)
     gates = 4 * parts
     units = 6 * parts
-    chunk = rows // parts
+    chunk = gu_all.shape[1] // parts
 
     z, y = fs_at // 2, fs_at % 2
     side = z // 2
@@ -113,6 +112,15 @@
     mate = tp_at + 1 - 2 * (tp_at % 2)
     diagonal = across + 1 - 2 * (tp_at % 2)
 
+    stages = [
+        pltpu.make_async_copy(src, dst, stage_sem.at[k])
+        for k, (src, dst) in enumerate(
+            [(gate_in, gate_stage), (up_in, up_stage), (down_in, down_stage), (tokens_in, tokens_ref)]
+        )
+    ]
+    for stage in stages:
+        stage.start()
+
     MESH = pl.DeviceIdType.MESH
     barrier = pltpu.get_barrier_semaphore()
 
@@ -127,67 +135,122 @@
         greet({"fs": E})
         greet({"fs": R})
         greet({"fs": X})
-        pl.semaphore_wait(barrier, tp_count + 2)
 
     @pl.when(end)
     def _():
         greet({"fs": M})
         greet({"fs": Eo})
-        pl.semaphore_wait(barrier, tp_count + 1)
+
+    own_cols = pl.ds(pl.multiple_of(fs_at * rows, rows), rows)
+    own_rows = pl.ds(pl.multiple_of((fs_at % 2) * down_rows, down_rows), down_rows)
+    for kind, stage in ((0, gate_stage), (1, up_stage)):
+        stages[kind].wait()
+        for p in range(4):
+            for i in (0, 1):
+                value = (stage[base[p] + i] * gain_ref[...]).astype(jnp.bfloat16)
+                top = (p % 2) * 384 + i * 128
+                low_at = (p % 2) * 384 + 256 + i * 64
+                gu_all[2 * (p // 2) + kind, pl.ds(top, 128), own_cols] = value[:128]
+                gu_all[2 * (p // 2) + kind, pl.ds(low_at, 64), own_cols] = value[128:]
+    stages[2].wait()
+    for p in range(4):
+        for i in (0, 1):
+            dn_all[p, fs_at // 2, i, own_rows, :] = down_stage[base[p] + i].astype(jnp.bfloat16)
+    meta_ref[pl.ds(0, 2), :] = ids_ref[...].astype(jnp.float32)
+    meta_ref[pl.ds(2, 2), :] = routes_ref[...]
+    meta_ref[pl.ds(4, 4), :] = jnp.zeros((4, tok_rows), jnp.float32)
+    pl.semaphore_wait(barrier, jnp.where(mid, tp_count + 2, tp_count + 1))
+
+    def is_down(u):
+        turn = jnp.logical_and(u >= 3 * parts, u % 2 == 0)
+        return jnp.logical_or(turn, u >= 5 * parts)
+
+    def is_wide(u):
+        return jnp.logical_or(jnp.logical_and(u >= parts, u % 2 == 1), u >= 5 * parts)
+
+    def gate_at(u):
+        turn = parts * (1 + u % 2) + (u - parts) // 2
+        return jnp.where(u < parts, u, jnp.where(u < 3 * parts, turn, (u + 3 * parts) // 2))
+
+    def down_at(u):
+        return jnp.where(u < 5 * parts, (u - 3 * parts) // 2, u - 4 * parts)
+
+    def wide_at(w):
+        return jnp.where(w < 2 * parts, parts + 1 + 2 * w, 3 * parts + w)
 
     def gu_view(u, s):
-        return gu_all.at[u // parts, pl.ds(pl.multiple_of(s * rows + (u % parts) * chunk, chunk), chunk), :]
-
-    def gu_own(u):
-        return gu_ref.at[u // parts, pl.ds(pl.multiple_of((u % parts) * chunk, chunk), chunk), :]
+        g = gate_at(u)
+        return gu_all.at[
+            g // parts,
+            pl.ds(pl.multiple_of((g % parts) * chunk, chunk), chunk),
+            pl.ds(pl.multiple_of(s * rows, rows), rows),
+        ]
 
     def dn_view(u, s):
-        v = u - gates
+        v = down_at(u)
         span = pl.ds(pl.multiple_of((s % 2) * down_rows, down_rows), down_rows)
         if parts == 4:
             return dn_all.at[v // 2, s // 2, v % 2, span, :]
         return dn_all.at[v, s // 2, :, span, :]
 
-    def dn_own(u):
-        v = u - gates
-        return dn_ref.at[v // 2, v % 2] if parts == 4 else dn_ref.at[v]
-
-    def copy(view, u, s, to, slot, src=None):
+    def copy(view, u, s, to, slot):
         place = view(u, s)
         return pltpu.make_async_remote_copy(
-            src_ref=place if src is None else src, dst_ref=place,
+            src_ref=place, dst_ref=place,
             send_sem=send_sem.at[slot, u], recv_sem=recv_sem.at[s, u],
             device_id={"fs": to}, device_id_type=MESH,
         )
 
     def group(u, body):
-        @pl.when(jnp.logical_and(u >= 0, u < gates))
-        def _():
-            body(u, gu_view, gu_own, u >= 2 * parts)
-
-        @pl.when(jnp.logical_and(u >= gates, u < units))
-        def _():
-            body(u, dn_view, dn_own, u >= 5 * parts)
-
-    def sends(u):
-        def from_mid(u, view, own, wide):
-            copy(view, u, fs_at, R, 0, own(u)).start()
-            copy(view, u, fs_at, X, 3, own(u)).start()
-            pl.when(wide)(lambda: copy(view, u, fs_at, E, 6, own(u)).start())
-
-        def from_end(u, view, own, wide):
-            copy(view, u, fs_at, M, 0, own(u)).start()
-            copy(view, u, fs_at, Eo, 2, own(u)).start()
-
-        pl.when(mid)(lambda: group(u, from_mid))
-        pl.when(end)(lambda: group(u, from_end))
+        inside = jnp.logical_and(u >= 0, u < units)
+
+        @pl.when(jnp.logical_and(inside, jnp.logical_not(is_down(u))))
+        def _():
+            body(u, gu_view, is_wide(u))
+
+        @pl.when(jnp.logical_and(inside, is_down(u)))
+        def _():
+            body(u, dn_view, is_wide(u))
+
+    def to_far(u, view, wide):
+        copy(view, u, fs_at, R, 0).start()
+        copy(view, u, fs_at, X, 3).start()
+
+    def to_end(u, view, wide):
+        copy(view, u, fs_at, E, 6).start()
+
+    def to_mid(u, view, wide):
+        copy(view, u, fs_at, M, 0).start()
+
+    def to_other(u, view, wide):
+        copy(view, u, fs_at, Eo, 2).start()
+
+    def sends(t):
+        @pl.when(mid)
+        def _():
+            group(t + ahead, to_far)
+            pl.when(t < units // 2)(lambda: group(wide_at(t), to_end))
+
+        @pl.when(end)
+        def _():
+            group(t + 2, to_mid)
+            group(2 * t + 2, to_other)
+            group(2 * t + 3, to_other)
+
+    def opening(u):
+        pl.when(mid)(lambda: group(u, to_far))
+
+        @pl.when(jnp.logical_and(end, u < 2))
+        def _():
+            group(u, to_mid)
+            group(u, to_other)
 
     def got(view, u, s):
         copy(view, u, s, s, 0).wait_recv()
 
     token_parts = 2 * parts
     token_rows = tok_rows // tp_count // token_parts
-    token_from = 1
+    token_from = 3
 
     def token_copy(j, owner, kind, to):
         span = pl.ds(pl.multiple_of((owner * token_parts + j) * token_rows, token_rows), token_rows)
@@ -199,11 +262,11 @@
         )
 
     def tick(t):
-        sends(t + ahead)
+        sends(t)
 
         @pl.when(mid)
         def _():
-            def first(u, view, own, wide):
+            def first(u, view, wide):
                 got(view, u, E)
                 copy(view, u, E, X, 4).start()
                 got(view, u, X)
@@ -211,7 +274,7 @@
                 pl.when(wide)(lambda: copy(view, u, X, E, 7).start())
                 got(view, u, R)
 
-            def second(u, view, own, wide):
+            def second(u, view, wide):
                 got(view, u, Eo)
                 pl.when(u % 2 == 1)(lambda: copy(view, u, Eo, X, 5).start())
                 got(view, u, F)
@@ -220,9 +283,9 @@
                 got(view, u, Xo)
 
             group(t, first)
-            group(t - 1, second)
-            group(t - 2, lambda u, view, own, wide: got(view, u, Fo))
-            j = t - token_from - 1
+            group(t - lag, second)
+            group(t - 2 * lag, lambda u, view, wide: got(view, u, Fo))
+            j = t - token_from - 2
 
             @pl.when(jnp.logical_and(j >= 0, j < token_parts))
             def _():
@@ -239,36 +302,42 @@
 
         @pl.when(end)
         def _():
-            def first(u, view, own, wide):
+            def first(u, view, wide):
                 got(view, u, Eo)
                 copy(view, u, Eo, M, 1).start()
 
-                @pl.when(wide)
-                def _():
-                    got(view, u, M)
-                    copy(view, u, M, Eo, 3).start()
-
-            def second(u, view, own, wide):
+            def early(u, view, wide):
+                got(view, u, M)
+                copy(view, u, M, Eo, 3).start()
+
+            def second(u, view, wide):
                 @pl.when(wide)
                 def _():
                     got(view, u, X)
                     copy(view, u, X, Eo, 4).start()
-                    got(view, u, R)
-
-            def third(u, view, own, wide):
+
+            def third(u, view, wide):
                 @pl.when(wide)
                 def _():
                     got(view, u, F)
                     copy(view, u, F, Eo, 5).start()
                     got(view, u, Xo)
 
-            def fourth(u, view, own, wide):
+            def fourth(u, view, wide):
                 pl.when(wide)(lambda: got(view, u, Fo))
 
             group(t, first)
-            group(t - 1, second)
-            group(t - 2, third)
-            group(t - 3, fourth)
+            early_at = t - 2 * parts
+            pl.when(jnp.logical_and(early_at >= 0, early_at < units // 2))(
+                lambda: group(wide_at(early_at), early)
+            )
+            late_at = early_at - 2
+            pl.when(jnp.logical_and(late_at >= 0, late_at < units // 2))(
+                lambda: group(wide_at(late_at), lambda u, view, wide: got(view, u, R))
+            )
+            group(t - lag, second)
+            group(t - 2 * lag, third)
+            group(t - 3 * lag, fourth)
             j = t - token_from
 
             @pl.when(jnp.logical_and(j >= 0, j < token_parts))
@@ -287,16 +356,15 @@
 
         lax.fori_loop(first, last, step, 0)
 
-    loop(0, ahead, sends)
+    loop(0, ahead, opening)
     pl.when(end)(meta_copy.start)
-    gu_all[:, pl.ds(pl.multiple_of(fs_at * rows, rows), rows), :] = gu_ref[...]
-    dn_all[:, fs_at // 2, :, pl.ds(pl.multiple_of((fs_at % 2) * down_rows, down_rows), down_rows), :] = dn_ref[...]
 
     def columns(which, ref):
         for b in range(tok_rows // 128):
             cols[which, pl.ds(b * 128, 128), :] = jnp.transpose(ref[:, pl.ds(b * 128, 128)])
 
     columns(0, meta_ref)
+    stages[3].wait()
 
     lane = lax.broadcasted_iota(jnp.int32, (1, 384), 1)
     parity = jnp.where(lane < 256, lane // 128, (lane - 256) // 64).astype(jnp.float32)
@@ -311,8 +379,13 @@
         square = jnp.mean(tokens * tokens, axis=-1, keepdims=True)
         tokens = (tokens * lax.rsqrt(square + epsilon)).astype(jnp.bfloat16)
         ids = [cols[which, span, pl.ds(k, 1)] for k in (0, 1)]
-        gate = jnp.dot(tokens, gu_all[2 * phase], preferred_element_type=jnp.float32)
-        up = jnp.dot(tokens, gu_all[2 * phase + 1], preferred_element_type=jnp.float32)
+        gate, up = [
+            lax.dot_general(
+                tokens, gu_all[2 * phase + kind], (((1,), (1,)), ((), ())),
+                preferred_element_type=jnp.float32,
+            )
+            for kind in (0, 1)
+        ]
         hidden = gate / (1.0 + jnp.exp(-gate)) * up
         folded = []
         for k in (0, 1):
@@ -392,7 +465,7 @@
             device_id={"fs": E}, device_id_type=MESH,
         )
 
-    start = 2 * parts + 2
+    start = 3 * parts - 2 + 2 * lag
     loop(0, start, tick)
 
     @pl.when(end)
@@ -431,51 +504,66 @@
         @pl.when(mid)
         def _():
             share(t - start, 1, evaluate(t - start, far_tokens, 1, 0))
+            pl.when(t >= start + 3)(lambda: pass_on(t - start - 3, 1))
 
     loop(start, start + blocks, far_first)
+    shared = start + 3
     start = start + blocks
-    ready = max(start, gates + 3)
-    loop(start, ready, tick)
+
+    def far_passed(t):
+        tick(t)
+        pl.when(mid)(lambda: pass_on(t - shared, 1))
+
+    ready = max(start + 1, 5 * parts - 2 + 2 * lag)
+    loop(start, ready, far_passed)
     start = ready
 
     def served(part):
         span = pl.ds(pl.multiple_of(part * rows, rows), rows)
         phase = jnp.where(mid, 0, 1)
         for kind, out in ((0, serve_g), (1, serve_u)):
-            out[span, pl.ds(0, 128)] = gu_all[
-                2 * phase + kind, span, pl.ds(pl.multiple_of(side * 384 + y * 128, 128), 128)
+            out[pl.ds(0, 128), span] = gu_all[
+                2 * phase + kind, pl.ds(pl.multiple_of(side * 384 + y * 128, 128), 128), span
             ]
-            tail = gu_all[
-                2 * phase + kind, span, pl.ds(pl.multiple_of(side * 384 + 256, 128), 128)
-            ].astype(jnp.float32)
-            tail = jnp.where(y == 1, pltpu.roll(tail, 64, 1), tail)
-            out[span, pl.ds(128, 64)] = tail[:, :64].astype(jnp.bfloat16)
-
-    def own_second(t):
-        tick(t)
-        block = t - start
-        folded = evaluate(block, tokens_ref, 0, 1)
-        span = span_of(block)
-        share(block, 0, [folded[k] + fold[k, span, :] for k in (0, 1)])
-        pl.when(mid)(lambda: pass_on(block, 1))
-
-    loop(start, start + blocks, own_second)
-    start = start + blocks
+            out[pl.ds(128, 64), span] = gu_all[
+                2 * phase + kind, pl.ds(pl.multiple_of(side * 384 + 256 + y * 64, 64), 64), span
+            ]
+
+    replied = start
 
     def far_second(t):
-        tick(t)
-        block = t - start
-        pass_on(block, 0)
-
-        @pl.when(mid)
-        def _():
+        block = t - replied
+
+        @pl.when(jnp.logical_and(mid, block < blocks))
+        def _():
+            pl.when(t - shared < blocks)(lambda: pass_on(t - shared, 1))
             picked_up(block, 1)
             reply[span_of(block)] = project(block, 1, 0).astype(jnp.bfloat16)
             reply_copy(block).start()
 
-    loop(start, start + blocks, far_second)
-    start = start + blocks
-    loop(start, max(start, units + 3), tick)
+    def far_only(t):
+        tick(t)
+        far_second(t)
+
+    ready = max(start, 5 * parts - 1 + 3 * lag)
+    loop(start, ready, far_only)
+    start = ready
+
+    def own_second(t):
+        tick(t)
+
+        def evaluated(block):
+            folded = evaluate(block, tokens_ref, 0, 1)
+            span = span_of(block)
+            share(block, 0, [folded[k] + fold[k, span, :] for k in (0, 1)])
+
+        loop(2 * (t - start), 2 * (t - start) + 2, evaluated)
+        far_second(t)
+
+    loop(start, start + blocks // 2, own_second)
+    start = start + blocks // 2
+    ready = max(replied + blocks, units + 3 * lag)
+    loop(start, ready, far_only)
 
     pair = jnp.where(mid, side, 2 + side)
 
@@ -507,10 +595,13 @@
 
         mixed_ref[span, :] = (total[span, :] + project(block, 0, 1)).astype(jnp.bfloat16)
 
-    loop(0, blocks, finish)
+    def close(block):
+        pl.when(block < blocks)(lambda: pass_on(block, 0))
+        pl.when(block > 0)(lambda: finish(block - 1))
+
 
     def drained(u):
-        def from_mid(u, view, own, wide):
+        def from_mid(u, view, wide):
             for slot in (0, 1, 3, 4):
                 copy(view, u, fs_at, X, slot).wait_send()
             pl.when(u % 2 == 0)(lambda: copy(view, u, fs_at, X, 2).wait_send())
@@ -521,7 +612,7 @@
                 for slot in (6, 7, 8):
                     copy(view, u, fs_at, X, slot).wait_send()
 
-        def from_end(u, view, own, wide):
+        def from_end(u, view, wide):
             for slot in (0, 1, 2):
                 copy(view, u, fs_at, M, slot).wait_send()
 
@@ -533,7 +624,9 @@
         pl.when(mid)(lambda: group(u, from_mid))
         pl.when(end)(lambda: group(u, from_end))
 
-    loop(0, units, drained)
+    loop(0, 5 * parts, drained)
+    loop(0, blocks + 1, close)
+    loop(5 * parts, units, drained)
 
     @pl.when(mid)
     def _():
@@ -571,44 +664,30 @@
     down_rows, down_cols = down_train.shape[1:]
     n, tp_count = lax.axis_size("fs"), lax.axis_size("tp")
     tok_rows, width = tokens.shape
-    half, quarter = experts // 2, experts // 4
-    blocks, parts, ahead = 4, 4, 3
-
-    def paired(train):
-        value = (norm_gain[None, :, None] * train).astype(jnp.bfloat16)
-        value = jnp.concatenate([value[quarter:-quarter], value[:quarter], value[-quarter:]], axis=0)
-        value = value.transpose(1, 0, 2).reshape(rows, 2, 2, 2, cols)
-        value = jnp.concatenate(
-            [value[..., :128].reshape(rows, 2, 2, 256), value[..., 128:].reshape(rows, 2, 2, 128)],
-            axis=3,
-        )
-        return value.transpose(1, 0, 2, 3).reshape(2, rows, 768)
-
-    gate, up = paired(gate_train), paired(up_train)
-    gu = jnp.stack([gate, up], axis=1).reshape(4, rows, 768)
-    down = down_train.astype(jnp.bfloat16)
-    down = jnp.concatenate([down[quarter:-quarter], down[:quarter], down[-quarter:]], axis=0)
-    down = down.reshape(4, 2, down_rows, down_cols)
-    meta = jnp.concatenate(
-        [expert_ids.T.astype(jnp.float32), route_weights.T, jnp.zeros((4, tok_rows), jnp.float32)],
-        axis=0,
-    )
+    blocks, parts, ahead, lag = 4, 4, 5, 1
     vmem = pl.BlockSpec(memory_space=pltpu.VMEM)
     dma = pltpu.SemaphoreType.DMA
     bf16, f32 = jnp.bfloat16, jnp.float32
+    anywhere = pl.BlockSpec(memory_space=pltpu.HBM)
     units = 6 * parts
     gate_serve, up_serve, down_serve, mixed = pl.pallas_call(
-        functools.partial(ladder_kernel, n, tp_count, parts, ahead, blocks),
+        functools.partial(ladder_kernel, n, tp_count, parts, ahead, lag, blocks),
         out_shape=(
-            jax.ShapeDtypeStruct((width, cols), bf16),
-            jax.ShapeDtypeStruct((width, cols), bf16),
+            jax.ShapeDtypeStruct((cols, width), bf16),
+            jax.ShapeDtypeStruct((cols, width), bf16),
             jax.ShapeDtypeStruct((2 * down_rows, width), bf16),
             jax.ShapeDtypeStruct((tok_rows, down_cols), bf16),
         ),
-        in_specs=[vmem] * 4,
+        in_specs=[anywhere] * 3 + [vmem, anywhere, vmem, vmem],
         out_specs=(vmem,) * 4,
         scratch_shapes=[
-            pltpu.VMEM((4, width, 768), bf16),
+            pltpu.VMEM((experts, cols, rows), f32),
+            pltpu.VMEM((experts, cols, rows), f32),
+            pltpu.VMEM((experts, down_rows, down_cols), f32),
+            pltpu.VMEM((tok_rows, width), bf16),
+            pltpu.VMEM((8, tok_rows), f32),
+            dma((4,)),
+            pltpu.VMEM((4, 4 * cols, width), bf16),
             pltpu.VMEM((4, tp_count, 2, 2 * down_rows, down_cols), bf16),
             pltpu.VMEM((tok_rows, width), bf16),
             pltpu.VMEM((8, tok_rows), f32),
@@ -634,8 +713,11 @@
         compiler_params=pltpu.CompilerParams(
             collective_id=0, has_side_effects=True, vmem_limit_bytes=63 * 1024 * 1024
         ),
-    )(gu, down, tokens, meta)
-    return gate_serve[None], up_serve[None], down_serve[None], mixed
+    )(
+        gate_train.transpose(0, 2, 1), up_train.transpose(0, 2, 1), down_train,
+        norm_gain[None, :], tokens, expert_ids.T, route_weights.T,
+    )
+    return gate_serve.T[None], up_serve.T[None], down_serve[None], mixed
 
 
 def on_device(tokens, norm_gain, gate_train, up_train, down_train, expert_ids, route_weights):

time: 209 us -> 187 us (0.89)
  Pallas kernels: 191 us -> 182 us
  other arithmetic: 7.95 us -> 0 us
  local copies, waits for them, and re-layouts: 9.09 us -> 4.95 us
    pallas_call x1, Pallas kernels: 191 us -> 182 us  [laddered(): pl.pallas_call(functools.partial(ladder_kernel, n, tp_count, parts, ahead...]
    convert_element_type x3 -> x0, other arithmetic: 2.56 us -> none  [the longest x1 1.51 us: laddered(): down = down_train.astype(jnp.bfloat16)]
    concatenate x4 -> x0, other arithmetic: 2.54 us -> none  [the longest x1 1.38 us: laddered(): jnp.concatenate([expert_ids.T.astype(jnp.float32), route_weights.T, jnp.z...]
    unnamed x16 -> x10, local copies, waits for them, and re-layouts: 6.51 us -> 4.95 us
where the time goes in v2:
time: 187 us
  Pallas kernels  182 us (97%)
  local copies, waits for them, and re-layouts  4.95 us (3%)
    pallas_call x1, Pallas kernels, laddered(): pl.pallas_call(functools.partial(ladder_kernel, n, tp_count, parts, ahead...  182 us
    unnamed x10, local copies, waits for them, and re-layouts  4.95 us

profile of v2, /device:TPU:0, one launch (start us, length us, event | category | flops | bytes accessed | tf_op | source)
XLA Modules:
  0.0 187.1 jit_solution(9114782090520774783)
XLA Ops:
  0.6 181.5 %shard_map.102 = (bf16[192,2048]{1,0:T(8,128)(2,1)}, bf16[192,2048]{1,0:T(8,128)(2,1)}, bf16[192,2048]{1,0:T(8,128)(2,1)}, bf16[1024,512]{1,0:T(8,128)(2,1)}) custom-call(f32[8,192,256]{2,1,0:T(8,128)} %bitcast.12, f32[8,192,256]{2,1,0:T(8,128)} %bitcast.13, f32[8,96,512]{2,1,0:T(8,128)} %down_in.1, f32[1,256]{1,0:T(1,128)} %bitcast.19, ...), custom_call_target="tpu_custom_call" | custom-call | tf_op jit(solution)/shard_map/pallas_call | solution.py:673
  182.2 0.0 copy-start.2
  182.2 0.0 copy-start.1
  182.2 2.2 %copy.15 = bf16[1,2048,192]{1,2,0:T(8,128)(2,1)} copy(bf16[1,2048,192]{1,2,0:T(8,128)(2,1)} %bitcast.16) | data formatting | bytes 1572864
  184.4 0.0 copy-done.2
  184.4 0.0 copy-start
  184.4 0.9 copy.16
  185.3 0.0 copy-done.1
  185.3 0.9 copy.17
  186.2 0.0 copy-done
  186.2 1.0 copy.18
Async XLA Ops:
  182.2 2.2 %copy-start.2 = (bf16[192,2048]{1,0:T(8,128)(2,1)S(1)}, bf16[192,2048]{1,0:T(8,128)(2,1)}, u32[]{:S(2)}) copy-start(bf16[192,2048]{1,0:T(8,128)(2,1)} %get-tuple-element.9) | copy-start | bytes 2359300
  182.2 3.1 %copy-start.1 = (bf16[192,2048]{1,0:T(8,128)(2,1)S(1)}, bf16[192,2048]{1,0:T(8,128)(2,1)}, u32[]{:S(2)}) copy-start(bf16[192,2048]{1,0:T(8,128)(2,1)} %get-tuple-element.10) | copy-start | bytes 2359300
  184.4 1.8 copy-start

commit v3 on v2

--- a/solution.py
+++ b/solution.py
@@ -93,6 +93,7 @@
     gates = 4 * parts
     units = 6 * parts
     chunk = gu_all.shape[1] // parts
+    flight = send_sem.shape[1]
 
     z, y = fs_at // 2, fs_at % 2
     side = z // 2
@@ -197,10 +198,18 @@
         place = view(u, s)
         return pltpu.make_async_remote_copy(
             src_ref=place, dst_ref=place,
-            send_sem=send_sem.at[slot, u], recv_sem=recv_sem.at[s, u],
+            send_sem=send_sem.at[slot, u % flight], recv_sem=recv_sem.at[s, u],
             device_id={"fs": to}, device_id_type=MESH,
         )
 
+    def launch(view, u, s, to, slot, wide_only=False):
+        due = u >= flight
+        if wide_only:
+            due = jnp.logical_and(due, is_wide(u - flight))
+        transfer = copy(view, u, s, to, slot)
+        pl.when(due)(transfer.wait_send)
+        transfer.start()
+
     def group(u, body):
         inside = jnp.logical_and(u >= 0, u < units)
 
@@ -213,17 +222,17 @@
             body(u, dn_view, is_wide(u))
 
     def to_far(u, view, wide):
-        copy(view, u, fs_at, R, 0).start()
-        copy(view, u, fs_at, X, 3).start()
+        launch(view, u, fs_at, R, 0)
+        launch(view, u, fs_at, X, 3)
 
     def to_end(u, view, wide):
-        copy(view, u, fs_at, E, 6).start()
+        launch(view, u, fs_at, E, 6, True)
 
     def to_mid(u, view, wide):
-        copy(view, u, fs_at, M, 0).start()
+        launch(view, u, fs_at, M, 0)
 
     def to_other(u, view, wide):
-        copy(view, u, fs_at, Eo, 2).start()
+        launch(view, u, fs_at, Eo, 2)
 
     def sends(t):
         @pl.when(mid)
@@ -237,6 +246,13 @@
             group(2 * t + 2, to_other)
             group(2 * t + 3, to_other)
 
+    def got(view, u, s):
+        copy(view, u, s, s, 0).wait_recv()
+
+    def up_from_other(u, view, wide):
+        got(view, u, Eo)
+        launch(view, u, Eo, M, 1)
+
     def opening(u):
         pl.when(mid)(lambda: group(u, to_far))
 
@@ -244,9 +260,6 @@
         def _():
             group(u, to_mid)
             group(u, to_other)
-
-    def got(view, u, s):
-        copy(view, u, s, s, 0).wait_recv()
 
     token_parts = 2 * parts
     token_rows = tok_rows // tp_count // token_parts
@@ -268,18 +281,18 @@
         def _():
             def first(u, view, wide):
                 got(view, u, E)
-                copy(view, u, E, X, 4).start()
+                launch(view, u, E, X, 4)
                 got(view, u, X)
-                copy(view, u, X, R, 1).start()
-                pl.when(wide)(lambda: copy(view, u, X, E, 7).start())
+                launch(view, u, X, R, 1)
+                pl.when(wide)(lambda: launch(view, u, X, E, 7, True))
                 got(view, u, R)
 
             def second(u, view, wide):
                 got(view, u, Eo)
-                pl.when(u % 2 == 1)(lambda: copy(view, u, Eo, X, 5).start())
+                pl.when(u % 2 == 1)(lambda: launch(view, u, Eo, X, 5))
                 got(view, u, F)
-                pl.when(u % 2 == 0)(lambda: copy(view, u, F, R, 2).start())
-                pl.when(wide)(lambda: copy(view, u, F, E, 8).start())
+                pl.when(u % 2 == 0)(lambda: launch(view, u, F, R, 2))
+                pl.when(wide)(lambda: launch(view, u, F, E, 8, True))
                 got(view, u, Xo)
 
             group(t, first)
@@ -302,31 +315,27 @@
 
         @pl.when(end)
         def _():
-            def first(u, view, wide):
-                got(view, u, Eo)
-                copy(view, u, Eo, M, 1).start()
-
             def early(u, view, wide):
                 got(view, u, M)
-                copy(view, u, M, Eo, 3).start()
+                launch(view, u, M, Eo, 3, True)
 
             def second(u, view, wide):
                 @pl.when(wide)
                 def _():
                     got(view, u, X)
-                    copy(view, u, X, Eo, 4).start()
+                    launch(view, u, X, Eo, 4, True)
 
             def third(u, view, wide):
                 @pl.when(wide)
                 def _():
                     got(view, u, F)
-                    copy(view, u, F, Eo, 5).start()
+                    launch(view, u, F, Eo, 5, True)
                     got(view, u, Xo)
 
             def fourth(u, view, wide):
-                pl.when(wide)(lambda: got(view, u, Fo))
-
-            group(t, first)
+                pl.when(jnp.logical_and(wide, u != 5 * parts - 1))(lambda: got(view, u, Fo))
+
+            group(t + 2, up_from_other)
             early_at = t - 2 * parts
             pl.when(jnp.logical_and(early_at >= 0, early_at < units // 2))(
                 lambda: group(wide_at(early_at), early)
@@ -465,6 +474,8 @@
             device_id={"fs": E}, device_id_type=MESH,
         )
 
+    pl.when(end)(lambda: loop(0, 2, lambda u: group(u, up_from_other)))
+
     start = 3 * parts - 2 + 2 * lag
     loop(0, start, tick)
 
@@ -514,7 +525,7 @@
         tick(t)
         pl.when(mid)(lambda: pass_on(t - shared, 1))
 
-    ready = max(start + 1, 5 * parts - 2 + 2 * lag)
+    ready = max(start, 5 * parts - 2 + 2 * lag)
     loop(start, ready, far_passed)
     start = ready
 
@@ -532,15 +543,19 @@
     replied = start
 
     def far_second(t):
-        block = t - replied
-
-        @pl.when(jnp.logical_and(mid, block < blocks))
-        def _():
-            pl.when(t - shared < blocks)(lambda: pass_on(t - shared, 1))
+        pl.when(jnp.logical_and(mid, t - shared < blocks))(lambda: pass_on(t - shared, 1))
+        early = t - replied
+        late = t - units
+
+        def replying(block):
             picked_up(block, 1)
             reply[span_of(block)] = project(block, 1, 0).astype(jnp.bfloat16)
             reply_copy(block).start()
 
+        first = jnp.where(early == 0, 0, 1)
+        count = jnp.where(early == 0, 1, jnp.where(late == 0, blocks - 1, 0))
+        pl.when(mid)(lambda: loop(first, first + count, replying))
+
     def far_only(t):
         tick(t)
         far_second(t)
@@ -549,20 +564,23 @@
     loop(start, ready, far_only)
     start = ready
 
+    pl.when(end)(
+        lambda: group(jnp.int32(5 * parts - 1), lambda u, view, wide: got(view, u, Fo))
+    )
+
     def own_second(t):
-        tick(t)
-
         def evaluated(block):
             folded = evaluate(block, tokens_ref, 0, 1)
             span = span_of(block)
             share(block, 0, [folded[k] + fold[k, span, :] for k in (0, 1)])
 
         loop(2 * (t - start), 2 * (t - start) + 2, evaluated)
+        tick(t)
         far_second(t)
 
     loop(start, start + blocks // 2, own_second)
     start = start + blocks // 2
-    ready = max(replied + blocks, units + 3 * lag)
+    ready = units + 3 * lag
     loop(start, ready, far_only)
 
     pair = jnp.where(mid, side, 2 + side)
@@ -584,16 +602,18 @@
         span = span_of(block)
         picked_up(block, 0)
 
+        total[span, :] = project(block, 0, 1)
+
         @pl.when(mid)
         def _():
-            total[span, :] = project(block, 0, 0)
+            mixed_ref[span, :] = (total[span, :] + project(block, 0, 0)).astype(jnp.bfloat16)
 
         @pl.when(end)
         def _():
             reply_copy(block).wait_recv()
-            total[span, :] = answer[span, :].astype(jnp.float32)
-
-        mixed_ref[span, :] = (total[span, :] + project(block, 0, 1)).astype(jnp.bfloat16)
+            mixed_ref[span, :] = (total[span, :] + answer[span, :].astype(jnp.float32)).astype(
+                jnp.bfloat16
+            )
 
     def close(block):
         pl.when(block < blocks)(lambda: pass_on(block, 0))
@@ -624,9 +644,8 @@
         pl.when(mid)(lambda: group(u, from_mid))
         pl.when(end)(lambda: group(u, from_end))
 
-    loop(0, 5 * parts, drained)
     loop(0, blocks + 1, close)
-    loop(5 * parts, units, drained)
+    loop(units - flight, units, drained)
 
     @pl.when(mid)
     def _():
@@ -697,7 +716,7 @@
             pltpu.VMEM((tok_rows, down_cols), f32),
             pltpu.VMEM((tok_rows, down_cols), bf16),
             pltpu.VMEM((tok_rows, down_cols), bf16),
-            dma((9, units)),
+            dma((9, 2 * parts)),
             dma((n, units)),
             dma((3, 2 * parts)),
             dma((tp_count, 2 * parts)),
@@ -711,7 +730,7 @@
             dma((tp_count,)),
         ],
         compiler_params=pltpu.CompilerParams(
-            collective_id=0, has_side_effects=True, vmem_limit_bytes=63 * 1024 * 1024
+            collective_id=0, has_side_effects=True, vmem_limit_bytes=50 * 1024 * 1024
         ),
     )(
         gate_train.transpose(0, 2, 1), up_train.transpose(0, 2, 1), down_train,

time: 187 us -> 178 us (0.952)
  Pallas kernels: 182 us -> 171 us
    pallas_call x1, Pallas kernels: 182 us -> 171 us  [laddered(): pl.pallas_call(functools.partial(ladder_kernel, n, tp_count, parts, ahead...]
where the time goes in v3:
time: 178 us; the launch traced here: 177 us
  Pallas kernels  171 us (96%)
  local copies, waits for them, and re-layouts  5.67 us (3%)
    pallas_call x1, Pallas kernels, laddered(): pl.pallas_call(functools.partial(ladder_kernel, n, tp_count, parts, ahead...  171 us
    unnamed x10, local copies, waits for them, and re-layouts  5.67 us

profile of v3, /device:TPU:0, one launch (start us, length us, event | category | flops | bytes accessed | tf_op | source)
XLA Modules:
  0.0 177.3 jit_solution(929175887861823995)
XLA Ops:
  0.6 0.0 copy-start
  0.6 0.7 copy-done
  1.3 0.0 copy-start.1
  1.3 0.7 copy-done.1
  2.0 0.0 copy-start.2
  2.0 0.7 copy-done.2
  2.7 171.0 %shard_map.102 = (bf16[192,2048]{1,0:T(8,128)(2,1)S(1)}, bf16[192,2048]{1,0:T(8,128)(2,1)S(1)}, bf16[192,2048]{1,0:T(8,128)(2,1)S(1)}, bf16[1024,512]{1,0:T(8,128)(2,1)S(1)}) custom-call(f32[8,192,256]{2,1,0:T(8,128)} %bitcast.18, f32[8,192,256]{2,1,0:T(8,128)} %bitcast.19, f32[8,96,512]{2,1,0:T(8,128)} %down_in.1, f32[1,256]{1,0:T(1,128)S(1)} %bitcast.17, ...), custom_call_target="tpu_custom_call" | custom-call | tf_op jit(solution)/shard_map/pallas_call | solution.py:692
  173.7 0.9 copy.15
  174.6 0.9 copy.16
  175.4 0.9 copy.17
  176.3 1.0 copy.18
Async XLA Ops:
  0.6 0.7 copy-start
  1.3 0.7 copy-start.1
  2.0 0.7 copy-start.2

commit v4 on v3

--- a/solution.py
+++ b/solution.py
@@ -676,6 +676,16 @@
         to = (tp_at + hop) % tp_count
         serve_copy(to, tp_at).wait_send()
         serve_copy(tp_at, to).wait_recv()
+
+
+def store_kernel(*refs):
+    copies = [
+        pltpu.make_async_copy(refs[k], refs[4 + k], refs[8].at[k]) for k in range(4)
+    ]
+    for copy in copies:
+        copy.start()
+    for copy in copies:
+        copy.wait()
 
 
 def laddered(tokens, norm_gain, gate_train, up_train, down_train, expert_ids, route_weights):
@@ -736,6 +746,15 @@
         gate_train.transpose(0, 2, 1), up_train.transpose(0, 2, 1), down_train,
         norm_gain[None, :], tokens, expert_ids.T, route_weights.T,
     )
+    results = (gate_serve, up_serve, down_serve, mixed)
+    gate_serve, up_serve, down_serve, mixed = pl.pallas_call(
+        store_kernel,
+        out_shape=tuple(jax.ShapeDtypeStruct(r.shape, r.dtype) for r in results),
+        in_specs=[pl.BlockSpec(memory_space=pl.ANY)] * 4,
+        out_specs=(anywhere,) * 4,
+        scratch_shapes=[dma((4,))],
+        compiler_params=pltpu.CompilerParams(vmem_limit_bytes=1024 * 1024),
+    )(*results)
     return gate_serve.T[None], up_serve.T[None], down_serve[None], mixed
 
 

time: 178 us -> 176 us (0.989)
  local copies, waits for them, and re-layouts: 5.67 us -> 2.06 us
  Pallas kernels: 171 us -> 173 us
    unnamed x10 -> x6, local copies, waits for them, and re-layouts: 5.67 us -> 2.06 us
    pallas_call x0 -> x1, Pallas kernels: none -> 1.78 us  [laddered(): pl.pallas_call(store_kernel, out_shape=tuple((jax.ShapeDtypeStruct(r.shap...]
where the time goes in v4:
time: 176 us
  Pallas kernels  173 us (98%)
  local copies, waits for them, and re-layouts  2.06 us (1%)
    pallas_call x1, Pallas kernels, laddered(): pl.pallas_call(functools.partial(ladder_kernel, n, tp_count, parts, ahead...  171 us

profile of v4, /device:TPU:0, one launch (start us, length us, event | category | flops | bytes accessed | tf_op | source)
XLA Modules:
  0.0 175.6 jit_solution(17961123026246172675)
XLA Ops:
  0.6 0.0 copy-start
  0.6 0.7 copy-done
  1.3 0.0 copy-start.1
  1.3 0.7 copy-done.1
  2.0 0.0 copy-start.2
  2.0 0.7 copy-done.2
  2.7 171.0 %shard_map.102 = (bf16[192,2048]{1,0:T(8,128)(2,1)S(1)}, bf16[192,2048]{1,0:T(8,128)(2,1)S(1)}, bf16[192,2048]{1,0:T(8,128)(2,1)S(1)}, bf16[1024,512]{1,0:T(8,128)(2,1)S(1)}) custom-call(f32[8,192,256]{2,1,0:T(8,128)} %bitcast.15, f32[8,192,256]{2,1,0:T(8,128)} %bitcast.16, f32[8,96,512]{2,1,0:T(8,128)} %down_in.1, f32[1,256]{1,0:T(1,128)S(1)} %bitcast.14, ...), custom_call_target="tpu_custom_call" | custom-call | tf_op jit(solution)/shard_map/pallas_call | solution.py:702
  173.7 1.8 %shard_map.103 = (bf16[192,2048]{1,0:T(8,128)(2,1)}, bf16[192,2048]{1,0:T(8,128)(2,1)}, bf16[192,2048]{1,0:T(8,128)(2,1)}, bf16[1024,512]{1,0:T(8,128)(2,1)}) custom-call(bf16[192,2048]{1,0:T(8,128)(2,1)S(1)} %get-tuple-element.12.refs_0_, bf16[192,2048]{1,0:T(8,128)(2,1)S(1)} %get-tuple-element.13.refs_1_, bf16[192,2048]{1,0:T(8,128)(2,1)S(1)} %get-tuple-element.14.refs_2_, ...), custom_call_target="tpu_custom_call" | custom-call | tf_op jit(solution)/shard_map/pallas_call | solution.py:750
Async XLA Ops:
  0.6 0.7 copy-start
  1.3 0.7 copy-start.1
  2.0 0.7 copy-start.2
